TPU v7x, 32 devices: a whole 2x2x4 slice. The times are simulated.
32 devices in a mesh: sp: 4 (over z), tp: 8 (over y, x, core).
Axes of the slice: x: 2, y: 2, z: 4, core: 2. Of those that a mesh axis runs over, the one named last changes fastest.
Arguments:
- target: bfloat16 [512, 2048], P('sp'), may hold values from -6 to 6
- source: bfloat16 [1024, 2048], P(('sp', 'tp')), may hold values from -6 to 6
- cotangent: bfloat16 [512, 2048], P('sp'), may hold values from -6 to 6
- target_gain: float32 [2048], replicated, may hold values from 0.1 to 1.9
- source_gain: float32 [2048], replicated, may hold values from 0.1 to 1.9
- query_weight: bfloat16 [2048, 8192], P(None, 'tp'), may hold values from -4 to 4
- key_weight: bfloat16 [2048, 2048], P(None, 'tp'), may hold values from -1 to 1
- value_projection_weight: bfloat16 [2048, 2048], P(None, 'tp'), may hold values from -0.125 to 0.125
- output_weight: bfloat16 [8192, 2048], P('tp'), may hold values from -0.0625 to 0.0625
Outputs:
- target_grad: float32 [512, 2048], P(('sp', 'tp'))
- source_grad: float32 [1024, 2048], P(('sp', 'tp'))
- key_weight_grad: float32 [2048, 2048], P(None, 'tp')
All inputs are finite; a program needn't handle non-finite values.
Results may differ from a plain program's by a relative error of at most 0.018.
The roundings to bfloat16 on the way count: a program that leaves them out, or rounds other values in their place, can miss the bound.
Values may be sent and summed in bfloat16 or wider, within the bound.
A program may use at most 64 MiB of HBM per device.

v0:
```python
import jax
import jax.numpy as jnp
from jax import lax
from jax.sharding import PartitionSpec as P

HEAD_SIZE = 256
EPSILON = 1e-05


def as_sent(array):

    def short(part):
        return part.astype(jnp.bfloat16) if part.dtype == jnp.float32 else part

    return jax.tree.map(short, array)


def partner_2(value, axis, bit):
    mask = 2**bit
    pairs = [(source, source ^ mask) for source in range(lax.axis_size(axis))]
    return lax.ppermute(value, axis, pairs)


def combined_all(value, axis, join):
    pieces = jax.tree.map(lambda part: lax.all_gather(part, axis), value)
    head = jax.tree.map(lambda part: part[0], pieces)
    tail = jax.tree.map(lambda part: part[1:], pieces)
    running, _ = lax.scan(lambda running, piece: (join(running, piece), None), head, tail)
    return running


def norm_rows(rows):
    values = rows.astype(jnp.float32)
    centred = values - jnp.mean(values, axis=-1, keepdims=True)
    inverse = lax.rsqrt(jnp.mean(centred * centred, axis=-1, keepdims=True) + EPSILON)
    return (centred * inverse, inverse)


def norm_back(scaled, inverse, gain, upstream):
    weighted = upstream * gain
    spread = jnp.mean(weighted * scaled, axis=-1, keepdims=True)
    return inverse * (weighted - jnp.mean(weighted, axis=-1, keepdims=True) - scaled * spread)


def times_transposed(left, right):
    return lax.dot_general(
        left, right, (((1,), (1,)), ((), ())), preferred_element_type=jnp.float32
    )


def split_heads(flat):
    return flat.reshape(flat.shape[0], flat.shape[1] // HEAD_SIZE, HEAD_SIZE)


def head_scores(queries, key_rows):
    return jnp.einsum(
        "rhd,sd->hrs", queries, key_rows, preferred_element_type=jnp.float32
    ) * HEAD_SIZE ** (-0.5)


def block_statistics(queries, out_grads, key_rows, value_rows):
    scores = head_scores(queries, key_rows)
    highest = jnp.max(scores, axis=2)
    weights = jnp.exp(scores - highest[:, :, None])
    products = jnp.einsum("rhd,sd->hrs", out_grads, value_rows, preferred_element_type=jnp.float32)
    return (highest, jnp.sum(weights, axis=2), jnp.sum(weights * products, axis=2))


def combine_statistics(former, latter):
    highest = jnp.maximum(former[0], latter[0])
    early_scale = jnp.exp(former[0] - highest)
    late_scale = jnp.exp(latter[0] - highest)
    return (
        highest,
        former[1] * early_scale + latter[1] * late_scale,
        former[2] * early_scale + latter[2] * late_scale,
    )


def score_grads(queries, out_grads, key_rows, value_rows, log_total, drifts):
    scores = head_scores(queries, key_rows)
    softmax_weights = jnp.exp(scores - log_total[:, :, None])
    products = jnp.einsum("rhd,sd->hrs", out_grads, value_rows, preferred_element_type=jnp.float32)
    slopes = (softmax_weights * (products - drifts[:, :, None]) * HEAD_SIZE ** (-0.5)).astype(
        jnp.bfloat16
    )
    return (softmax_weights.astype(jnp.bfloat16), slopes)


def join_heads(stacked):
    position = lax.axis_index("tp")
    part_cols = stacked.shape[2]
    bit_level = 0
    while part_cols < HEAD_SIZE:
        partner = jax.tree.map(
            lambda part, own: part.astype(own.dtype),
            partner_2(as_sent(stacked), "tp", bit_level),
            stacked,
        )
        upper_half = position >> bit_level & 1
        stacked = jnp.where(
            upper_half == 0,
            jnp.concatenate((stacked, partner), 2),
            jnp.concatenate((partner, stacked), 2),
        )
        part_cols = part_cols * 2
        bit_level = bit_level + 1
    return stacked


def split_sums(stacked, part_cols):
    position = lax.axis_index("tp")
    bit_count = (HEAD_SIZE // part_cols).bit_length() - 1
    for bit_level in reversed(range(bit_count)):
        half_cols = stacked.shape[2] // 2
        lower_half = stacked[:, :, :half_cols]
        upper_cols = stacked[:, :, half_cols:]
        upper_half = position >> bit_level & 1
        kept_half = jnp.where(upper_half == 0, lower_half, upper_cols)
        sent_half = jnp.where(upper_half == 0, upper_cols, lower_half)
        stacked = kept_half + partner_2(sent_half, "tp", bit_level)
    return stacked


def on_device(
    target,
    source,
    cotangent,
    target_gain,
    source_gain,
    query_weight,
    key_weight,
    value_projection_weight,
    output_weight,
):
    part_cols = key_weight.shape[1]
    src_scaled, src_inverse = norm_rows(source)
    src_normed = (src_scaled * source_gain).astype(jnp.bfloat16)
    tgt_scaled, tgt_inverse = norm_rows(target)
    tgt_normed = (tgt_scaled * target_gain).astype(jnp.bfloat16)
    block_rows = lax.all_gather(src_normed, "tp", axis=0, tiled=True)
    key_portion = jnp.dot(block_rows, key_weight, preferred_element_type=jnp.float32).astype(
        jnp.bfloat16
    )
    value_part = jnp.dot(
        block_rows, value_projection_weight, preferred_element_type=jnp.float32
    ).astype(jnp.bfloat16)
    parted = jnp.stack((key_portion, value_part))
    queries = split_heads(
        jnp.dot(tgt_normed, query_weight, preferred_element_type=jnp.float32).astype(jnp.bfloat16)
    )
    out_grads = split_heads(times_transposed(cotangent, output_weight).astype(jnp.bfloat16))
    head_count = queries.shape[1]
    own_rows = queries.shape[0]
    own_keys = join_heads(parted)
    all_queries, all_grads = (
        lax.all_gather(queries, "sp", axis=0, tiled=True),
        lax.all_gather(out_grads, "sp", axis=0, tiled=True),
    )
    partial_value = block_statistics(all_queries, all_grads, own_keys[0], own_keys[1])
    highest, totals, weighted = combined_all(partial_value, "sp", combine_statistics)
    log_total = highest + jnp.log(totals)
    drifts = weighted / totals
    attention, slopes = score_grads(
        all_queries, all_grads, own_keys[0], own_keys[1], log_total, drifts
    )
    key_gradient_rows = jnp.einsum(
        "hrs,rhd->sd", slopes, all_queries, preferred_element_type=jnp.float32
    )
    value_gradient_rows = jnp.einsum(
        "hrs,rhd->sd", attention, all_grads, preferred_element_type=jnp.float32
    )
    row_start = lax.axis_index("sp") * own_rows
    own_log = lax.dynamic_slice_in_dim(log_total, row_start, own_rows, 1)
    own_drifts = lax.dynamic_slice_in_dim(drifts, row_start, own_rows, 1)
    pieces = lax.all_gather(own_keys, "sp", axis=1, tiled=True)
    unused, slopes = score_grads(queries, out_grads, pieces[0], pieces[1], own_log, own_drifts)
    query_grads = jnp.einsum("hrs,sd->rhd", slopes, pieces[0], preferred_element_type=jnp.float32)
    summed = split_sums(jnp.stack((key_gradient_rows, value_gradient_rows)), part_cols)
    key_flattened = summed[0].astype(jnp.bfloat16)
    value_flattened = summed[1].astype(jnp.bfloat16)
    weight_part = lax.dot_general(
        block_rows, key_flattened, (((0,), (0,)), ((), ())), preferred_element_type=jnp.float32
    )
    key_weight_grad = lax.psum(weight_part.astype(jnp.bfloat16), "sp").astype(jnp.float32)
    source_upstream = lax.psum_scatter(
        (
            times_transposed(key_flattened, key_weight)
            + times_transposed(value_flattened, value_projection_weight)
        ).astype(jnp.bfloat16),
        "tp",
        scatter_dimension=0,
        tiled=True,
    ).astype(jnp.float32)
    source_grad = norm_back(src_scaled, src_inverse, source_gain, source_upstream)
    query_flat = query_grads.astype(jnp.bfloat16).reshape(own_rows, head_count * HEAD_SIZE)
    out_rows = own_rows // lax.axis_size("tp")
    out_start = lax.axis_index("tp") * out_rows
    target_upstream = lax.psum_scatter(
        times_transposed(query_flat, query_weight), "tp", scatter_dimension=0, tiled=True
    )
    slice_scaled = lax.dynamic_slice_in_dim(tgt_scaled, out_start, out_rows, 0)
    slice_inverse = lax.dynamic_slice_in_dim(tgt_inverse, out_start, out_rows, 0)
    slice_cotangent = lax.dynamic_slice_in_dim(cotangent, out_start, out_rows, 0)
    target_grad = slice_cotangent.astype(jnp.float32) + norm_back(
        slice_scaled, slice_inverse, target_gain, target_upstream
    )
    return (target_grad, source_grad, key_weight_grad)


def solution(mesh):
    return jax.shard_map(
        on_device,
        mesh=mesh,
        in_specs=(
            P("sp", None),
            P(("sp", "tp"), None),
            P("sp", None),
            P(),
            P(),
            P(None, "tp"),
            P(None, "tp"),
            P(None, "tp"),
            P("tp", None),
        ),
        out_specs=(P(("sp", "tp"), None), P(("sp", "tp"), None), P(None, "tp")),
        check_vma=False,
    )
```

profile of v0, /device:TPU:0, one launch (start us, length us, event | category | flops | bytes accessed | tf_op | source)
XLA Modules:
  0.0 308.4 jit_solution(17943720126214287300)
XLA Ops:
  7.2 1.1 convert_reduce_fusion.1
  8.3 1.1 fusion.46
  9.5 1.7 fusion.42
  11.2 1.2 convert_reduce_fusion
  12.4 1.3 fusion.22
  13.8 3.2 %convolution_convert_fusion.2 = bf16[128,1024]{1,0:T(8,128)(2,1)S(1)} fusion(bf16[2048,1024]{1,0:T(8,128)(2,1)} %param.16, f32[2048]{0:T(1024)} %param.14, bf16[128,2048]{1,0:T(8,128)(2,1)} %param.11, f32[128]{0:T(128)S(1)} %add_rsqrt_fusion.1, f32[128]{0:T(128)S(1)} %broadcast_multiply_fusion.5), kind=kOutput, calls=%fused_computation.38 | convolution fusion | flops 538312704 | bytes 4989952 | tf_op jit(solution)/shard_map/dot_general | solution.py:150
  18.5 3.7 %convolution_convert_fusion.1 = bf16[128,1024]{1,0:T(8,128)(2,1)S(1)} fusion(bf16[128,2048]{1,0:T(8,128)(2,1)S(1)} %copy-done.9, bf16[1024,2048]{1,0:T(8,128)(2,1)} %param.19), kind=kOutput, calls=%fused_computation.37 | convolution fusion | flops 537001984 | bytes 4980736 | tf_op jit(solution)/shard_map/dot_general | solution.py:46
  23.7 13.7 %all-gather.11.cloned.1.call-done = bf16[256,2048]{1,0:T(8,128)(2,1)} async-done(((bf16[32,2048]{1,0:T(8,128)(2,1)}), bf16[256,2048]{1,0:T(8,128)(2,1)}) %all-gather.11.cloned.1.call-update) | async-done | bytes 1048592 | tf_op jit(solution)/shard_map/all_gather | solution.py:141
  37.4 1.7 convolution_convert_fusion.4
  39.7 27.9 %all-gather.15.cloned.1.call-done = bf16[512,4,256]{2,0,1:T(8,128)(2,1)} async-done(((bf16[128,4,256]{2,0,1:T(8,128)(2,1)}), bf16[512,4,256]{2,0,1:T(8,128)(2,1)}) %all-gather.15.cloned.1.call-update) | async-done | bytes 1048592 | tf_op jit(solution)/shard_map/all_gather | solution.py:157
  67.6 1.7 bitcast_reduce_fusion
  69.3 27.8 %all-gather.17.cloned.1.call-done = bf16[512,4,256]{2,0,1:T(8,128)(2,1)} async-done(((bf16[128,4,256]{2,0,1:T(8,128)(2,1)}), bf16[512,4,256]{2,0,1:T(8,128)(2,1)}) %all-gather.17.cloned.1.call-update) | async-done | bytes 1048592 | tf_op jit(solution)/shard_map/all_gather | solution.py:158
  97.1 3.1 fusion.7
  100.2 13.1 %all-gather.5 = f32[4,4,512]{2,1,0:T(4,128)S(1)} all-gather(f32[1,4,512]{2,1,0:T(4,128)S(1)} %bitcast.163), channel_id=4, replica_groups=mesh['sp'=4,'tp'=8] {'sp'}, dimensions={0}, use_global_device_ids=true | all-gather | bytes 40960 | tf_op jit(solution)/shard_map/all_gather | solution.py:25
  113.3 13.1 %all-gather.4 = f32[4,4,512]{2,1,0:T(4,128)S(1)} all-gather(f32[1,4,512]{2,1,0:T(4,128)S(1)} %bitcast.162), channel_id=3, replica_groups=mesh['sp'=4,'tp'=8] {'sp'}, dimensions={0}, use_global_device_ids=true | all-gather | bytes 40960 | tf_op jit(solution)/shard_map/all_gather | solution.py:25
  126.5 13.1 %all-gather.3 = f32[4,4,512]{2,1,0:T(4,128)S(1)} all-gather(f32[1,4,512]{2,1,0:T(4,128)S(1)} %bitcast.161), channel_id=2, replica_groups=mesh['sp'=4,'tp'=8] {'sp'}, dimensions={0}, use_global_device_ids=true | all-gather | bytes 40960 | tf_op jit(solution)/shard_map/all_gather | solution.py:25
  140.7 2.5 fusion.20
  143.3 1.5 convolution_convert_fusion
  144.8 1.8 fusion.55
  146.6 4.6 %fusion.3 = bf16[256,2048]{1,0:T(8,128)(2,1)} fusion(f32[256,2048]{1,0:T(8,128)} %fusion.55, bf16[2048,256]{1,0:T(8,128)(2,1)} %param.18, bf16[512,4,256]{2,0,1:T(8,128)(2,1)} %all-gather.17.cloned.1.call-done, f32[256,512,4]{1,0,2:T(8,128)S(1)} %get-tuple-element.70, f32[4,512]{1,0:T(4,128)S(1)} %get-tuple-element.67), kind=kOutput, calls=%fused_computation.9 | convolution fusion | flops 539033600 | bytes 7348224 | tf_op jit(solution)/shard_map/dot_general | solution.py:46
  151.3 16.6 %all-gather.13.cloned.1.call-done = bf16[2,1024,256]{2,1,0:T(8,128)(2,1)} async-done(((bf16[2,256,256]{2,1,0:T(8,128)(2,1)}), bf16[2,1024,256]{2,1,0:T(8,128)(2,1)}) %all-gather.13.cloned.1.call-update) | async-done | bytes 1048592 | tf_op jit(solution)/shard_map/all_gather | solution.py:176
  167.9 1.6 fusion.36
  169.5 2.9 fusion.19
  172.4 4.8 %fusion.54 = f32[128,2048]{1,0:T(8,128)} fusion(bf16[128,1024]{0,1:T(8,128)(2,1)} %bitcast.160, bf16[2048,1024]{1,0:T(8,128)(2,1)} %param.16), kind=kOutput, calls=%fused_computation.98 | convolution fusion | flops 536870912 | bytes 5505024 | tf_op jit(solution)/shard_map/dot_general | solution.py:46
  177.7 43.8 %all-reduce.2.cloned.1.call-done = bf16[2048,256]{1,0:T(8,128)(2,1)} async-done(((bf16[2048,256]{1,0:T(8,128)(2,1)}), bf16[2048,256]{1,0:T(8,128)(2,1)}) %all-reduce.2.cloned.1.call-update) | async-done | bytes 1048592 | tf_op jit(solution)/shard_map/psum | solution.py:185
  221.4 2.7 convert_element_type.79
  224.1 35.6 %reduce-scatter.5.cloned.1.call-done = bf16[32,2048]{1,0:T(8,128)(2,1)} async-done(((bf16[256,2048]{1,0:T(8,128)(2,1)}), bf16[32,2048]{1,0:T(8,128)(2,1)}) %reduce-scatter.5.cloned.1.call-update) | async-done | bytes 131088 | tf_op jit(solution)/shard_map/reduce_scatter | solution.py:186
  259.7 1.1 fusion.47
  260.9 1.7 fusion.45
  262.6 36.3 %reduce-scatter.3.cloned.1.call-done = f32[16,2048]{1,0:T(8,128)} async-done(((f32[128,2048]{1,0:T(8,128)}), f32[16,2048]{1,0:T(8,128)}) %reduce-scatter.3.cloned.1.call-update) | async-done | bytes 131088 | tf_op jit(solution)/shard_map/reduce_scatter | solution.py:199
  298.9 1.0 multiply_reduce_fusion.1
  299.9 1.7 multiply_add_fusion
  (69 shorter events, 5.4 us)
Async XLA Ops:
  7.2 30.3 %copy-start = (bf16[2048,256]{1,0:T(8,128)(2,1)S(1)}, bf16[2048,256]{1,0:T(8,128)(2,1)}, u32[]{:S(2)}) copy-start(bf16[2048,256]{1,0:T(8,128)(2,1)} %param.17) | copy-start | bytes 3145732
  7.2 30.2 %all-gather.11.cloned.1.call-start = ((), (), s32[]{:S(2)}) async-start(), calls=%async_computation.2 | async-start | bytes 1179648 | tf_op jit(solution)/shard_map/all_gather | solution.py:141
  11.2 56.4 %all-gather.15.cloned.1.call-start = ((), (), s32[]{:S(2)}) async-start(), calls=%async_computation.4 | async-start | bytes 1310720 | tf_op jit(solution)/shard_map/all_gather | solution.py:157
  13.8 4.7 %copy-start.9 = (bf16[128,2048]{1,0:T(8,128)(2,1)S(1)}, bf16[128,2048]{1,0:T(8,128)(2,1)}, u32[]{:S(2)}) copy-start(bf16[128,2048]{1,0:T(8,128)(2,1)} %param.13) | copy-start | bytes 1572868
  17.0 0.7 copy-start.8
  18.4 78.7 %all-gather.17.cloned.1.call-start = ((), (), s32[]{:S(2)}) async-start(), calls=%async_computation.5 | async-start | bytes 1310720 | tf_op jit(solution)/shard_map/all_gather | solution.py:158
  22.2 0.7 copy-start.6
  22.2 17.0 %copy-start.4 = (bf16[2048,256]{1,0:T(8,128)(2,1)S(1)}, bf16[2048,256]{1,0:T(8,128)(2,1)}, u32[]{:S(2)}) copy-start(bf16[2048,256]{1,0:T(8,128)(2,1)} %param.18) | copy-start | bytes 3145732
  23.7 144.2 %all-gather.13.cloned.1.call-start = ((), (), s32[]{:S(2)}) async-start(), calls=%async_computation.3 | async-start | bytes 1310720 | tf_op jit(solution)/shard_map/all_gather | solution.py:176
  37.4 1.8 copy-start.1
  140.4 81.1 %all-reduce.2.cloned.1.call-start = ((), (), s32[]{:S(2)}) async-start(), calls=%async_computation.8 | async-start | bytes 2097152 | tf_op jit(solution)/shard_map/psum | solution.py:185
  140.7 2.6 copy-start.2
  144.8 115.0 %reduce-scatter.5.cloned.1.call-start = ((), (), s32[]{:S(2)}) async-start(), calls=%async_computation.7 | async-start | bytes 1179648 | tf_op jit(solution)/shard_map/reduce_scatter | solution.py:186
  151.2 18.2 %copy-start.7 = (bf16[128,1024]{1,0:T(8,128)(2,1)S(1)}, bf16[128,1024]{1,0:T(8,128)(2,1)}, u32[]{:S(2)}) copy-start(bf16[128,1024]{1,0:T(8,128)(2,1)} %copy-done.6) | copy-start | bytes 786436
  151.2 147.6 %reduce-scatter.3.cloned.1.call-start = ((), (), s32[]{:S(2)}) async-start(), calls=%async_computation.6 | async-start | bytes 1179648 | tf_op jit(solution)/shard_map/reduce_scatter | solution.py:199
  172.4 5.0 %copy-start.3 = (bf16[128,2048]{1,0:T(8,128)(2,1)S(1)}, bf16[128,2048]{1,0:T(8,128)(2,1)}, u32[]{:S(2)}) copy-start(bf16[128,2048]{1,0:T(8,128)(2,1)} %param.11) | copy-start | bytes 1572868
  177.3 82.4 %copy-start.5 = (bf16[32,2048]{1,0:T(8,128)(2,1)S(1)}, bf16[32,2048]{1,0:T(8,128)(2,1)}, u32[]{:S(2)}) copy-start(bf16[32,2048]{1,0:T(8,128)(2,1)} %param.12) | copy-start | bytes 393220
  177.3 82.4 %copy-start.10 = (f32[2048]{0:T(1024)S(1)}, f32[2048]{0:T(1024)}, u32[]{:S(2)}) copy-start(f32[2048]{0:T(1024)} %param.15) | copy-start | bytes 24580
  177.6 121.2 %copy-start.11 = (f32[2048]{0:T(1024)S(1)}, f32[2048]{0:T(1024)}, u32[]{:S(2)}) copy-start(f32[2048]{0:T(1024)} %param.14) | copy-start | bytes 24580
Sparse Core Ops, SparseCore 0:
  11.3 26.0 all-gather.10
  39.6 27.9 all-gather.14
  69.7 27.3 all-gather.16
  140.5 27.3 all-gather.12
  170.1 51.2 all-reduce.1
  224.4 35.2 reduce-scatter.4
  262.9 35.9 reduce-scatter.2
where the time goes:
time: 309 us; the launch traced here: 308 us
  waiting for transfers between devices  202 us (65%)
  blocking collectives  39.4 us (13%)
  matrix products  33.6 us (11%)
  other arithmetic  16 us (5%)
  between operations  14.3 us (5%)
    psum x1, waiting for transfers between devices, on_device(): lax.psum(weight_part.astype(jnp.bfloat16), 'sp').astype(jnp.float32)  43.8 us
    all_gather x3, blocking collectives, combined_all(): pieces = jax.tree.map(lambda part: lax.all_gather(part, axis), value)  39.4 us
    reduce_scatter x1, waiting for transfers between devices, on_device(): lax.psum_scatter(times_transposed(query_flat, query_weight), 'tp', scatte...  36.3 us
    reduce_scatter x1, waiting for transfers between devices, on_device(): lax.psum_scatter((times_transposed(key_flattened, key_weight) + times_tra...  35.6 us
    all_gather x1, waiting for transfers between devices, on_device(): lax.all_gather(queries, 'sp', axis=0, tiled=True)  27.9 us
    all_gather x1, waiting for transfers between devices, on_device(): lax.all_gather(out_grads, 'sp', axis=0, tiled=True)  27.8 us
    all_gather x1, waiting for transfers between devices, on_device(): pieces = lax.all_gather(own_keys, 'sp', axis=1, tiled=True)  16.6 us
    dot_general x4, matrix products, times_transposed(): lax.dot_general(left, right, (((1,), (1,)), ((), ())), preferred_element_...  15 us
  transfers between devices with their start and end apart: 7, of which 7 were waited for; matrix products, arithmetic and copies ran while one was open for 13% of the time, Pallas kernels for 0%

commit v1 on v0

--- a/solution.py
+++ b/solution.py
@@ -173,7 +173,12 @@
     row_start = lax.axis_index("sp") * own_rows
     own_log = lax.dynamic_slice_in_dim(log_total, row_start, own_rows, 1)
     own_drifts = lax.dynamic_slice_in_dim(drifts, row_start, own_rows, 1)
-    pieces = lax.all_gather(own_keys, "sp", axis=1, tiled=True)
+    ring = [own_keys]
+    for hop in range(3):
+        ring.append(lax.ppermute(ring[-1], "sp", [(dev, (dev + 1) % 4) for dev in range(4)]))
+    pieces = jnp.roll(
+        jnp.concatenate(ring[::-1], axis=1), (lax.axis_index("sp") + 1) * ring[0].shape[1], axis=1
+    )
     unused, slopes = score_grads(queries, out_grads, pieces[0], pieces[1], own_log, own_drifts)
     query_grads = jnp.einsum("hrs,sd->rhd", slopes, pieces[0], preferred_element_type=jnp.float32)
     summed = split_sums(jnp.stack((key_gradient_rows, value_gradient_rows)), part_cols)

time: 309 us -> 289 us (0.935)
  waiting for transfers between devices: 202 us -> 178 us
  local copies, waits for them, and re-layouts: 3.01 us -> 8.38 us
    psum x1, waiting for transfers between devices: 43.8 us -> 7.68 us  [on_device(): lax.psum(weight_part.astype(jnp.bfloat16), 'sp').astype(jnp.float32)]
    ppermute x0 -> x3, waiting for transfers between devices: none -> 27.9 us  [on_device(): lax.ppermute(ring[-1], 'sp', [(dev, (dev + 1) % 4) for dev in range(4)])]
    all_gather x1 -> x0, waiting for transfers between devices: 16.6 us -> none  [on_device(): pieces = lax.all_gather(own_keys, 'sp', axis=1, tiled=True)]
    unnamed x24 -> x48, local copies, waits for them, and re-layouts: 1.46 us -> 6.77 us
  transfers between devices with their start and end apart: 7 -> 9, of which waited for: 7 -> 9; matrix products, arithmetic and copies ran while one was open for 13% -> 14% of each run, Pallas kernels for 0% -> 0%
where the time goes in v1:
time: 289 us; the launch traced here: 288 us
  waiting for transfers between devices  178 us (62%)
  blocking collectives  39.4 us (14%)
  matrix products  31.7 us (11%)
  other arithmetic  16 us (6%)
  between operations  14.5 us (5%)
  local copies, waits for them, and re-layouts  8.38 us (3%)
    all_gather x3, blocking collectives, combined_all(): pieces = jax.tree.map(lambda part: lax.all_gather(part, axis), value)  39.4 us
    reduce_scatter x1, waiting for transfers between devices, on_device(): lax.psum_scatter(times_transposed(query_flat, query_weight), 'tp', scatte...  36.1 us
    reduce_scatter x1, waiting for transfers between devices, on_device(): lax.psum_scatter((times_transposed(key_flattened, key_weight) + times_tra...  35.6 us
    all_gather x1, waiting for transfers between devices, on_device(): lax.all_gather(queries, 'sp', axis=0, tiled=True)  27.9 us
    ppermute x3, waiting for transfers between devices, on_device(): lax.ppermute(ring[-1], 'sp', [(dev, (dev + 1) % 4) for dev in range(4)])  27.9 us
    all_gather x1, waiting for transfers between devices, on_device(): lax.all_gather(out_grads, 'sp', axis=0, tiled=True)  27.8 us
    all_gather x1, waiting for transfers between devices, on_device(): block_rows = lax.all_gather(src_normed, 'tp', axis=0, tiled=True)  15 us
    dot_general x4, matrix products, times_transposed(): lax.dot_general(left, right, (((1,), (1,)), ((), ())), preferred_element_...  14.8 us
  transfers between devices with their start and end apart: 9, of which 9 were waited for; matrix products, arithmetic and copies ran while one was open for 14% of the time, Pallas kernels for 0%

profile of v1, /device:TPU:0, one launch (start us, length us, event | category | flops | bytes accessed | tf_op | source)
XLA Modules:
  0.0 288.4 jit_solution(16550787706448440743)
XLA Ops:
  7.2 1.1 convert_reduce_fusion.1
  8.4 1.1 fusion.46
  9.5 1.7 fusion.42
  11.2 1.2 convert_reduce_fusion
  12.4 1.3 fusion.22
  13.8 3.2 %convolution_convert_fusion.2 = bf16[128,1024]{1,0:T(8,128)(2,1)S(1)} fusion(bf16[2048,1024]{1,0:T(8,128)(2,1)} %param.16, f32[2048]{0:T(1024)} %param.14, bf16[128,2048]{1,0:T(8,128)(2,1)} %param.11, f32[128]{0:T(128)S(1)} %add_rsqrt_fusion.1, f32[128]{0:T(128)S(1)} %broadcast_multiply_fusion.5), kind=kOutput, calls=%fused_computation.38 | convolution fusion | flops 538312704 | bytes 4989952 | tf_op jit(solution)/shard_map/dot_general | solution.py:150
  17.9 3.7 %convolution_convert_fusion.1 = bf16[128,1024]{1,0:T(8,128)(2,1)S(1)} fusion(bf16[128,2048]{1,0:T(8,128)(2,1)S(1)} %copy-done.9, bf16[1024,2048]{1,0:T(8,128)(2,1)} %param.19), kind=kOutput, calls=%fused_computation.37 | convolution fusion | flops 537001984 | bytes 4980736 | tf_op jit(solution)/shard_map/dot_general | solution.py:46
  22.4 15.0 %all-gather.10.cloned.1.call-done = bf16[256,2048]{1,0:T(8,128)(2,1)} async-done(((bf16[32,2048]{1,0:T(8,128)(2,1)}), bf16[256,2048]{1,0:T(8,128)(2,1)}) %all-gather.10.cloned.1.call-update) | async-done | bytes 1048592 | tf_op jit(solution)/shard_map/all_gather | solution.py:141
  37.4 1.8 convolution_convert_fusion.4
  39.7 27.9 %all-gather.12.cloned.1.call-done = bf16[512,4,256]{2,0,1:T(8,128)(2,1)} async-done(((bf16[128,4,256]{2,0,1:T(8,128)(2,1)}), bf16[512,4,256]{2,0,1:T(8,128)(2,1)}) %all-gather.12.cloned.1.call-update) | async-done | bytes 1048592 | tf_op jit(solution)/shard_map/all_gather | solution.py:157
  67.6 1.7 bitcast_reduce_fusion
  69.3 27.8 %all-gather.14.cloned.1.call-done = bf16[512,4,256]{2,0,1:T(8,128)(2,1)} async-done(((bf16[128,4,256]{2,0,1:T(8,128)(2,1)}), bf16[512,4,256]{2,0,1:T(8,128)(2,1)}) %all-gather.14.cloned.1.call-update) | async-done | bytes 1048592 | tf_op jit(solution)/shard_map/all_gather | solution.py:158
  97.1 3.1 %fusion.7 = (f32[4,512]{1,0:T(4,128)S(1)}, f32[4,512]{1,0:T(4,128)S(1)}, f32[256,512,4]{1,0,2:T(8,128)}) fusion(f32[256,512,4]{1,0,2:T(8,128)S(1)} %get-tuple-element.70, f32[4,512]{1,0:T(4,128)S(1)} %get-tuple-element.69, bf16[512,4,256]{2,0,1:T(8,128)(2,1)} %all-gather.14.cloned.1.call-done, bf16[256,256]{1,0:T(8,128)(2,1)S(1)} %convolution_convert_fusion.3), kind=kOutput, calls=%fused_computation.17 | convolution fusion | flops 270528512 | bytes 5398528 | tf_op jit(solution)/shard_map/rhd,sd->hrs/dot_general | solution.py:65
  100.2 13.1 %all-gather.5 = f32[4,4,512]{2,1,0:T(4,128)S(1)} all-gather(f32[1,4,512]{2,1,0:T(4,128)S(1)} %bitcast.167), channel_id=4, replica_groups=mesh['sp'=4,'tp'=8] {'sp'}, dimensions={0}, use_global_device_ids=true | all-gather | bytes 40960 | tf_op jit(solution)/shard_map/all_gather | solution.py:25
  113.3 13.1 %all-gather.4 = f32[4,4,512]{2,1,0:T(4,128)S(1)} all-gather(f32[1,4,512]{2,1,0:T(4,128)S(1)} %bitcast.166), channel_id=3, replica_groups=mesh['sp'=4,'tp'=8] {'sp'}, dimensions={0}, use_global_device_ids=true | all-gather | bytes 40960 | tf_op jit(solution)/shard_map/all_gather | solution.py:25
  126.5 13.1 %all-gather.3 = f32[4,4,512]{2,1,0:T(4,128)S(1)} all-gather(f32[1,4,512]{2,1,0:T(4,128)S(1)} %bitcast.165), channel_id=2, replica_groups=mesh['sp'=4,'tp'=8] {'sp'}, dimensions={0}, use_global_device_ids=true | all-gather | bytes 40960 | tf_op jit(solution)/shard_map/all_gather | solution.py:25
  139.9 2.5 fusion.20
  142.5 1.5 convolution_convert_fusion
  144.7 9.3 %collective-permute-done = bf16[2,256,256]{2,1,0:T(8,128)(2,1)} collective-permute-done((bf16[2,256,256]{2,1,0:T(8,128)(2,1)}, bf16[2,256,256]{2,1,0:T(8,128)(2,1)}, u32[]{:S(2)}, u32[]{:S(2)}) %collective-permute-start) | collective-permute-done | bytes 262176 | tf_op jit(solution)/shard_map/ppermute | solution.py:178
  154.0 1.8 fusion.58
  155.8 13.5 %collective-permute-done.1 = bf16[2,256,256]{2,1,0:T(8,128)(2,1)} collective-permute-done((bf16[2,256,256]{2,1,0:T(8,128)(2,1)}, bf16[2,256,256]{2,1,0:T(8,128)(2,1)}, u32[]{:S(2)}, u32[]{:S(2)}) %collective-permute-start.1) | collective-permute-done | bytes 262176 | tf_op jit(solution)/shard_map/ppermute | solution.py:178
  169.3 4.5 %fusion.3 = bf16[256,2048]{1,0:T(8,128)(2,1)} fusion(f32[256,2048]{1,0:T(8,128)} %fusion.58, bf16[2048,256]{1,0:T(8,128)(2,1)} %param.18, bf16[512,4,256]{2,0,1:T(8,128)(2,1)} %all-gather.14.cloned.1.call-done, f32[256,512,4]{1,0,2:T(8,128)S(1)} %get-tuple-element.70, f32[4,512]{1,0:T(4,128)S(1)} %get-tuple-element.67), kind=kOutput, calls=%fused_computation.9 | convolution fusion | flops 539033600 | bytes 7348224 | tf_op jit(solution)/shard_map/dot_general | solution.py:46
  174.0 5.1 %collective-permute-done.2 = bf16[2,256,256]{2,1,0:T(8,128)(2,1)} collective-permute-done((bf16[2,256,256]{2,1,0:T(8,128)(2,1)}, bf16[2,256,256]{2,1,0:T(8,128)(2,1)}, u32[]{:S(2)}, u32[]{:S(2)}) %collective-permute-start.2) | collective-permute-done | bytes 262176 | tf_op jit(solution)/shard_map/ppermute | solution.py:178
  186.3 2.3 fusion.19
  188.6 4.8 %fusion.57 = f32[128,2048]{1,0:T(8,128)} fusion(bf16[128,1024]{0,1:T(8,128)(2,1)S(1)} %bitcast.164, bf16[2048,1024]{1,0:T(8,128)(2,1)} %param.16), kind=kOutput, calls=%fused_computation.108 | convolution fusion | flops 536870912 | bytes 5505024 | tf_op jit(solution)/shard_map/dot_general | solution.py:46
  193.8 7.7 %all-reduce.2.cloned.1.call-done = bf16[2048,256]{1,0:T(8,128)(2,1)} async-done(((bf16[2048,256]{1,0:T(8,128)(2,1)}), bf16[2048,256]{1,0:T(8,128)(2,1)}) %all-reduce.2.cloned.1.call-update) | async-done | bytes 1048592 | tf_op jit(solution)/shard_map/psum | solution.py:190
  201.5 2.7 convert_element_type.79
  204.2 35.6 %reduce-scatter.5.cloned.1.call-done = bf16[32,2048]{1,0:T(8,128)(2,1)} async-done(((bf16[256,2048]{1,0:T(8,128)(2,1)}), bf16[32,2048]{1,0:T(8,128)(2,1)}) %reduce-scatter.5.cloned.1.call-update) | async-done | bytes 131088 | tf_op jit(solution)/shard_map/reduce_scatter | solution.py:191
  239.8 1.1 fusion.47
  241.0 1.7 fusion.45
  242.7 36.1 %reduce-scatter.3.cloned.1.call-done = f32[16,2048]{1,0:T(8,128)} async-done(((f32[128,2048]{1,0:T(8,128)}), f32[16,2048]{1,0:T(8,128)}) %reduce-scatter.3.cloned.1.call-update) | async-done | bytes 131088 | tf_op jit(solution)/shard_map/reduce_scatter | solution.py:204
  279.9 1.7 multiply_add_fusion
  (98 shorter events, 12.2 us)
Async XLA Ops:
  7.2 30.3 %copy-start = (bf16[2048,256]{1,0:T(8,128)(2,1)S(1)}, bf16[2048,256]{1,0:T(8,128)(2,1)}, u32[]{:S(2)}) copy-start(bf16[2048,256]{1,0:T(8,128)(2,1)} %param.17) | copy-start | bytes 3145732
  7.2 30.3 %all-gather.10.cloned.1.call-start = ((), (), s32[]{:S(2)}) async-start(), calls=%async_computation.2 | async-start | bytes 1179648 | tf_op jit(solution)/shard_map/all_gather | solution.py:141
  8.3 5.4 %copy-start.13 = (f32[32]{0:T(128)}, f32[32]{0:T(128)S(1)}, u32[]{:S(2)}) copy-start(f32[32]{0:T(128)S(1)} %broadcast_multiply_fusion.4) | copy-start | bytes 388
  9.5 4.3 %copy-start.15 = (f32[32]{0:T(128)}, f32[32]{0:T(128)S(1)}, u32[]{:S(2)}) copy-start(f32[32]{0:T(128)S(1)} %add_rsqrt_fusion) | copy-start | bytes 388
  11.2 56.4 %all-gather.12.cloned.1.call-start = ((), (), s32[]{:S(2)}) async-start(), calls=%async_computation.3 | async-start | bytes 1310720 | tf_op jit(solution)/shard_map/all_gather | solution.py:157
  12.4 4.6 %copy-start.17 = (f32[128]{0:T(128)}, f32[128]{0:T(128)S(1)}, u32[]{:S(2)}) copy-start(f32[128]{0:T(128)S(1)} %broadcast_multiply_fusion.5) | copy-start | bytes 1540
  13.8 3.2 %copy-start.19 = (f32[128]{0:T(128)}, f32[128]{0:T(128)S(1)}, u32[]{:S(2)}) copy-start(f32[128]{0:T(128)S(1)} %add_rsqrt_fusion.1) | copy-start | bytes 1540
  13.8 4.1 %copy-start.9 = (bf16[128,2048]{1,0:T(8,128)(2,1)S(1)}, bf16[128,2048]{1,0:T(8,128)(2,1)}, u32[]{:S(2)}) copy-start(bf16[128,2048]{1,0:T(8,128)(2,1)} %param.13) | copy-start | bytes 1572868
  17.0 4.6 %copy-start.6 = (bf16[128,1024]{1,0:T(8,128)(2,1)}, bf16[128,1024]{1,0:T(8,128)(2,1)S(1)}, u32[]{:S(2)}) copy-start(bf16[128,1024]{1,0:T(8,128)(2,1)S(1)} %convolution_convert_fusion.2) | copy-start | bytes 786436
  17.8 79.3 %all-gather.14.cloned.1.call-start = ((), (), s32[]{:S(2)}) async-start(), calls=%async_computation.4 | async-start | bytes 1310720 | tf_op jit(solution)/shard_map/all_gather | solution.py:158
  21.6 0.8 copy-start.8
  21.6 17.6 %copy-start.4 = (bf16[2048,256]{1,0:T(8,128)(2,1)S(1)}, bf16[2048,256]{1,0:T(8,128)(2,1)}, u32[]{:S(2)}) copy-start(bf16[2048,256]{1,0:T(8,128)(2,1)} %param.18) | copy-start | bytes 3145732
  22.4 179.1 %all-reduce.2.cloned.1.call-start = ((), (), s32[]{:S(2)}) async-start(), calls=%async_computation.7 | async-start | bytes 2097152 | tf_op jit(solution)/shard_map/psum | solution.py:190
  37.4 1.8 copy-start.1
  139.9 2.6 copy-start.2
  144.0 95.8 %reduce-scatter.5.cloned.1.call-start = ((), (), s32[]{:S(2)}) async-start(), calls=%async_computation.6 | async-start | bytes 1179648 | tf_op jit(solution)/shard_map/reduce_scatter | solution.py:191
  144.7 9.3 %collective-permute-start = (bf16[2,256,256]{2,1,0:T(8,128)(2,1)}, bf16[2,256,256]{2,1,0:T(8,128)(2,1)}, u32[]{:S(2)}, u32[]{:S(2)}) collective-permute-start(bf16[2,256,256]{2,1,0:T(8,128)(2,1)} %pad_maximum_fusion), channel_id=1, source_target_pairs={{0,8},{8,16},{16,24},{24,0},{1,9},{9,17},{17,25},{25,1},{2,10},{10... | collective-permute-start | bytes 786440 | tf_op jit(solution)/shard_map/ppermute | solution.py:178
  154.0 15.3 %collective-permute-start.1 = (bf16[2,256,256]{2,1,0:T(8,128)(2,1)}, bf16[2,256,256]{2,1,0:T(8,128)(2,1)}, u32[]{:S(2)}, u32[]{:S(2)}) collective-permute-start(bf16[2,256,256]{2,1,0:T(8,128)(2,1)} %collective-permute-done), channel_id=1, source_target_pairs={{0,8},{8,16},{16,24},{24,0},{1,9},{9,17},{17,25},{25,1},{2,10},{10... | collective-permute-start | bytes 786440 | tf_op jit(solution)/shard_map/ppermute | solution.py:178
  169.3 9.7 %collective-permute-start.2 = (bf16[2,256,256]{2,1,0:T(8,128)(2,1)}, bf16[2,256,256]{2,1,0:T(8,128)(2,1)}, u32[]{:S(2)}, u32[]{:S(2)}) collective-permute-start(bf16[2,256,256]{2,1,0:T(8,128)(2,1)} %collective-permute-done.1), channel_id=1, source_target_pairs={{0,8},{8,16},{16,24},{24,0},{1,9},{9,17},{17,25},{25,1},{2,10},{10... | collective-permute-start | bytes 786440 | tf_op jit(solution)/shard_map/ppermute | solution.py:178
  173.9 105.0 %reduce-scatter.3.cloned.1.call-start = ((), (), s32[]{:S(2)}) async-start(), calls=%async_computation.5 | async-start | bytes 1179648 | tf_op jit(solution)/shard_map/reduce_scatter | solution.py:204
  173.9 11.0 %copy-start.7 = (bf16[128,1024]{1,0:T(8,128)(2,1)S(1)}, bf16[128,1024]{1,0:T(8,128)(2,1)}, u32[]{:S(2)}) copy-start(bf16[128,1024]{1,0:T(8,128)(2,1)} %copy-done.6) | copy-start | bytes 786436
  185.0 1.3 copy-start.10
  188.6 4.8 %copy-start.20 = (f32[128]{0:T(128)S(1)}, f32[128]{0:T(128)}, u32[]{:S(2)}) copy-start(f32[128]{0:T(128)} %copy-done.19) | copy-start | bytes 1540
  188.6 4.9 %copy-start.3 = (bf16[128,2048]{1,0:T(8,128)(2,1)S(1)}, bf16[128,2048]{1,0:T(8,128)(2,1)}, u32[]{:S(2)}) copy-start(bf16[128,2048]{1,0:T(8,128)(2,1)} %param.11) | copy-start | bytes 1572868
  188.6 4.9 %copy-start.18 = (f32[128]{0:T(128)S(1)}, f32[128]{0:T(128)}, u32[]{:S(2)}) copy-start(f32[128]{0:T(128)} %copy-done.17) | copy-start | bytes 1540
  193.5 46.3 %copy-start.5 = (bf16[32,2048]{1,0:T(8,128)(2,1)S(1)}, bf16[32,2048]{1,0:T(8,128)(2,1)}, u32[]{:S(2)}) copy-start(bf16[32,2048]{1,0:T(8,128)(2,1)} %param.12) | copy-start | bytes 393220
  193.5 46.3 %copy-start.11 = (f32[2048]{0:T(1024)S(1)}, f32[2048]{0:T(1024)}, u32[]{:S(2)}) copy-start(f32[2048]{0:T(1024)} %param.15) | copy-start | bytes 24580
  193.5 46.3 %copy-start.14 = (f32[32]{0:T(128)S(1)}, f32[32]{0:T(128)}, u32[]{:S(2)}) copy-start(f32[32]{0:T(128)} %copy-done.13) | copy-start | bytes 388
  193.5 46.3 %copy-start.16 = (f32[32]{0:T(128)S(1)}, f32[32]{0:T(128)}, u32[]{:S(2)}) copy-start(f32[32]{0:T(128)} %copy-done.15) | copy-start | bytes 388
  193.8 85.0 %copy-start.12 = (f32[2048]{0:T(1024)S(1)}, f32[2048]{0:T(1024)}, u32[]{:S(2)}) copy-start(f32[2048]{0:T(1024)} %param.14) | copy-start | bytes 24580
Sparse Core Ops, SparseCore 0:
  11.3 26.0 all-gather.9
  39.6 27.9 all-gather.11
  69.7 27.3 all-gather.13
  144.1 57.3 all-reduce.1
  204.5 35.2 reduce-scatter.4
  242.8 35.9 reduce-scatter.2
